TPU v7x, 32 devices: a whole 2x2x4 slice. The times are simulated.
32 devices in a mesh: fs: 8 (over z, y), tp: 4 (over x, core).
Axes of the slice: x: 2, y: 2, z: 4, core: 2. Of those that a mesh axis runs over, the one named last changes fastest.
Arguments:
- stream: bfloat16 [3072, 2048], P('fs', 'tp'), may hold values from -3 to 3
- gain_first: float32 [2048], replicated, may hold values from 0.1 to 1.9
- gain_mixer: float32 [2048], replicated, may hold values from 0.1 to 1.9
- gain_second: float32 [2048], replicated, may hold values from 0.1 to 1.9
- gate_weight: float32 [2048, 5632], P('fs', 'tp'), may hold values from -0.125 to 0.125
- gate_scale: float32 [5632], P('tp'), may hold values from 0.5 to 2
- up_weight: float32 [2048, 5632], P('fs', 'tp'), may hold values from -0.125 to 0.125
- up_scale: float32 [5632], P('tp'), may hold values from 0.5 to 2
- down_weight: float32 [5632, 2048], P('tp', 'fs'), may hold values from -0.109375 to 0.109375
- down_scale: float32 [2048], P('tp'), may hold values from 0.5 to 2
- pool_in_weight: float32 [2048, 512], P('fs', 'tp'), may hold values from -0.125 to 0.125
- pool_in_scale: float32 [512], P('tp'), may hold values from 0.5 to 2
- pool_out_weight: float32 [512, 2048], P('tp', 'fs'), may hold values from -0.375 to 0.375
- pool_out_scale: float32 [2048], P('tp'), may hold values from 0.5 to 2
Outputs:
- layer_out: bfloat16 [3072, 2048], P('fs', 'tp')
All inputs are finite; a program needn't handle non-finite values.
Results may differ from a plain program's by a relative error of at most 0.025.
Values may be sent and summed in bfloat16 or wider, within the bound.
A program may use at most 64 MiB of HBM per device.

v0:
```python
import jax
import jax.numpy as jnp
from jax import lax
from jax.sharding import PartitionSpec as P

SEQ = 128
eps = 1e-06
WINDOWS = (2, 4, 8, 16)


def normed(own_columns, norm_gain):
    gathered = lax.all_gather(own_columns, "tp", axis=1, tiled=True)
    floats = gathered.astype(jnp.float32)
    scaled = floats * lax.rsqrt(jnp.mean(floats * floats, axis=-1, keepdims=True) + eps)
    return (scaled * norm_gain).astype(jnp.bfloat16)


def residual_add(own_columns, partial_value, column_scale, factor):
    summed = lax.psum_scatter(
        partial_value.astype(jnp.bfloat16), "tp", scatter_dimension=1, tiled=True
    ).astype(jnp.float32)
    return (own_columns.astype(jnp.float32) + factor * (summed * column_scale)).astype(jnp.bfloat16)


def pooling(pool_input):
    channels = pool_input.shape[1]
    floats = pool_input.astype(jnp.float32).reshape(-1, SEQ, channels)
    csum = jnp.concatenate(
        [jnp.zeros((floats.shape[0], 1, channels), jnp.float32), jnp.cumsum(floats, axis=1)], axis=1
    )
    position = jnp.arange(SEQ)
    channel_index = lax.axis_index("tp") * channels + jnp.arange(channels, dtype=jnp.int32)
    channel_group = channel_index * 4 // (channels * lax.axis_size("tp"))
    pooled = -floats
    for group_index, window in enumerate(WINDOWS):
        before = window // 2
        after_span = window - before
        upper_sum = jnp.pad(csum, ((0, 0), (0, after_span), (0, 0)), mode="edge")[
            :, after_span : after_span + SEQ
        ]
        lower_sum = jnp.pad(csum, ((0, 0), (before, 0), (0, 0)), mode="edge")[:, :SEQ]
        counts = (
            jnp.minimum(position + after_span, SEQ) - jnp.maximum(position - before, 0)
        ).astype(jnp.float32)
        window_mean = (upper_sum - lower_sum) / counts[None, :, None]
        select = (channel_group == group_index).astype(jnp.float32)
        pooled = pooled + window_mean * select
    return pooled.reshape(-1, channels).astype(jnp.bfloat16)


def body(
    stream,
    gain_first,
    gain_mixer,
    gain_second,
    gate_weight,
    gate_scale,
    up_weight,
    up_scale,
    down_weight,
    down_scale,
    pool_in_weight,
    pool_in_scale,
    pool_out_weight,
    pool_out_scale,
):
    gate_half = gate_weight.astype(jnp.bfloat16)
    up_half = up_weight.astype(jnp.bfloat16)
    down_half = down_weight.astype(jnp.bfloat16)
    in_half = pool_in_weight.astype(jnp.bfloat16)
    out_half = pool_out_weight.astype(jnp.bfloat16)
    in_whole, out_whole = (
        lax.all_gather(in_half, "fs", axis=0, tiled=True),
        lax.all_gather(out_half, "fs", axis=1, tiled=True),
    )
    gate_whole, up_whole, down_whole = (
        lax.all_gather(gate_half, "fs", axis=0, tiled=True),
        lax.all_gather(up_half, "fs", axis=0, tiled=True),
        lax.all_gather(down_half, "fs", axis=1, tiled=True),
    )

    def feed_forward(normed_rows):
        gate_sum = jnp.dot(normed_rows, gate_whole, preferred_element_type=jnp.float32) * gate_scale
        up_sum = jnp.dot(normed_rows, up_whole, preferred_element_type=jnp.float32) * up_scale
        hidden = (jax.nn.silu(gate_sum) * up_sum).astype(jnp.bfloat16)
        return jnp.dot(hidden, down_whole, preferred_element_type=jnp.float32)

    after_first = residual_add(stream, feed_forward(normed(stream, gain_first)), down_scale, 0.5)
    mixer_normed = normed(after_first, gain_mixer)
    pool_input = (
        jnp.dot(mixer_normed, in_whole, preferred_element_type=jnp.float32) * pool_in_scale
    ).astype(jnp.bfloat16)
    pooled = pooling(pool_input)
    tp_count = lax.axis_size("tp")
    all_pooled = lax.all_gather(pooled, "tp", axis=1, tiled=True)
    out_columns = lax.all_to_all(out_whole, "tp", split_axis=1, concat_axis=0, tiled=True)
    block_width = out_columns.shape[0] // tp_count
    pooled_blocks = all_pooled.reshape(all_pooled.shape[0], tp_count, block_width)
    weight_blocks = out_columns.reshape(tp_count, block_width, out_columns.shape[1])
    partials = jnp.einsum(
        "rbc,bcd->brd", pooled_blocks, weight_blocks, preferred_element_type=jnp.float32
    ).astype(jnp.bfloat16)
    mixed = jnp.sum(partials.astype(jnp.float32), axis=0)
    after_mix = (after_first.astype(jnp.float32) + mixed * pool_out_scale).astype(jnp.bfloat16)
    return residual_add(after_mix, feed_forward(normed(after_mix, gain_second)), down_scale, 0.5)


def solution(mesh):
    placed = (
        P("fs", "tp"),
        P(),
        P(),
        P(),
        P("fs", "tp"),
        P("tp"),
        P("fs", "tp"),
        P("tp"),
        P("tp", "fs"),
        P("tp"),
        P("fs", "tp"),
        P("tp"),
        P("tp", "fs"),
        P("tp"),
    )
    return jax.shard_map(body, mesh=mesh, in_specs=placed, out_specs=P("fs", "tp"), check_vma=False)
```

profile of v0, /device:TPU:0, one launch (start us, length us, event | category | flops | bytes accessed | tf_op | source)
XLA Modules:
  0.0 509.7 jit_solution(2998391872795220859)
XLA Ops:
  7.3 2.3 convert_element_type.144
  11.2 1.0 convert_element_type.147
  12.3 19.0 %all-gather.7.cloned.1.call-done = bf16[384,2048]{1,0:T(8,128)(2,1)} async-done(((bf16[384,512]{1,0:T(8,128)(2,1)}), bf16[384,2048]{1,0:T(8,128)(2,1)}) %all-gather.7.cloned.1.call-update) | async-done | bytes 1572880 | tf_op jit(solution)/shard_map/all_gather | solution.py:12
  31.3 1.8 fusion
  33.1 92.7 %all-gather.9.cloned.1.call-done = bf16[2048,1408]{1,0:T(8,128)(2,1)} async-done(((bf16[256,1408]{1,0:T(8,128)(2,1)}), bf16[2048,1408]{1,0:T(8,128)(2,1)}) %all-gather.9.cloned.1.call-update) | async-done | bytes 5767184 | tf_op jit(solution)/shard_map/all_gather | solution.py:77
  125.8 7.1 %convolution_multiply_fusion.3 = f32[384,1408]{1,0:T(8,128)} fusion(bf16[2048,1408]{1,0:T(8,128)(2,1)} %all-gather.9.cloned.1.call-done, f32[1408]{0:T(1024)S(1)} %copy-done.13, bf16[384,2048]{1,0:T(8,128)(2,1)} %all-gather.7.cloned.1.call-done, f32[2048]{0:T(1024)S(1)} %copy-done.11, f32[384]{0:T(512)S(1)} %add_rsqrt_fusion.2), kind=kOutput, calls=%fused_computation.21 | convolution fusion | flops 2218278912 | bytes 9518080 | tf_op jit(solution)/shard_map/dot_general | solution.py:83
  133.0 85.6 %all-gather.11.cloned.1.call-done = bf16[2048,1408]{1,0:T(8,128)(2,1)} async-done(((bf16[256,1408]{1,0:T(8,128)(2,1)}), bf16[2048,1408]{1,0:T(8,128)(2,1)}) %all-gather.11.cloned.1.call-update) | async-done | bytes 5767184 | tf_op jit(solution)/shard_map/all_gather | solution.py:78
  218.5 93.2 %all-gather.13.cloned.1.call-done = bf16[1408,2048]{1,0:T(8,128)(2,1)} async-done(((bf16[1408,256]{1,0:T(8,128)(2,1)}), bf16[1408,2048]{1,0:T(8,128)(2,1)}) %all-gather.13.cloned.1.call-update) | async-done | bytes 5767184 | tf_op jit(solution)/shard_map/all_gather | solution.py:79
  311.8 11.2 %convolution_convert_fusion.1 = bf16[384,2048]{1,0:T(8,128)(2,1)} fusion(bf16[1408,2048]{1,0:T(8,128)(2,1)} %all-gather.13.cloned.1.call-done, bf16[2048,1408]{1,0:T(8,128)(2,1)} %all-gather.11.cloned.1.call-done, f32[384,1408]{1,0:T(8,128)} %convolution_multiply_fusion.3, f32[1408]{0:T(1024)S(1)} %copy-done.14, bf16[384,2048]{1,0:T(8,128)(2,1)S(1)} %copy-done.2, ...), kind=kOutput, calls=%fused_computation.23 | convolution fusion | flops 4436901888 | bytes 16858112 | tf_op jit(solution)/shard_map/dot_general | solution.py:86
  323.1 26.3 %reduce-scatter.3.cloned.1.call-done = bf16[384,512]{1,0:T(8,128)(2,1)} async-done(((bf16[384,2048]{1,0:T(8,128)(2,1)}), bf16[384,512]{1,0:T(8,128)(2,1)}) %reduce-scatter.3.cloned.1.call-update) | async-done | bytes 393232 | tf_op jit(solution)/shard_map/reduce_scatter | solution.py:19
  349.3 1.9 add_convert_fusion.2
  351.4 31.7 %all_gather.34 = bf16[128,2048]{0,1:T(8,128)(2,1)S(1)} all-gather(bf16[128,256]{0,1:T(8,128)(2,1)S(1)} %copy.16), channel_id=1, replica_groups=mesh['fs'=8,'tp'=4] {'fs'}, dimensions={1}, use_global_device_ids=true | all-gather | bytes 589824 | tf_op jit(solution)/shard_map/all_gather | solution.py:74
  383.1 1.0 copy.17
  384.1 3.5 all-to-all-start
  387.8 31.5 %all_gather.32 = bf16[2048,128]{1,0:T(8,128)(2,1)S(1)} all-gather(bf16[256,128]{1,0:T(8,128)(2,1)S(1)} %convert_element_type.154), channel_id=1, replica_groups=mesh['fs'=8,'tp'=4] {'fs'}, dimensions={0}, use_global_device_ids=true | all-gather | bytes 589824 | tf_op jit(solution)/shard_map/all_gather | solution.py:73
  419.3 1.8 fusion.3
  421.1 2.0 fusion.20
  423.9 6.7 %all_gather.33 = bf16[384,512]{0,1:T(8,128)(2,1)S(1)} all-gather(bf16[384,128]{0,1:T(8,128)(2,1)S(1)} %copy.15), channel_id=1, replica_groups=mesh['fs'=8,'tp'=4] {'tp'}, dimensions={1}, use_global_device_ids=true | all-gather | bytes 491520 | tf_op jit(solution)/shard_map/all_gather | solution.py:95
  432.4 20.1 %all-gather.17.cloned.1.call-done = bf16[384,2048]{1,0:T(8,128)(2,1)} async-done(((bf16[384,512]{1,0:T(8,128)(2,1)}), bf16[384,2048]{1,0:T(8,128)(2,1)}) %all-gather.17.cloned.1.call-update) | async-done | bytes 1572880 | tf_op jit(solution)/shard_map/all_gather | solution.py:12
  452.4 1.8 fusion.6
  454.3 7.2 %convolution_multiply_fusion.1 = f32[384,1408]{1,0:T(8,128)} fusion(bf16[2048,1408]{1,0:T(8,128)(2,1)} %all-gather.9.cloned.1.call-done, f32[1408]{0:T(1024)S(1)} %copy-done.13, bf16[384,2048]{1,0:T(8,128)(2,1)} %all-gather.17.cloned.1.call-done, f32[2048]{0:T(1024)S(1)} %copy-done.15, f32[384]{0:T(512)S(1)} %add_rsqrt_fusion), kind=kOutput, calls=%fused_computation.18 | convolution fusion | flops 2218278912 | bytes 9518080 | tf_op jit(solution)/shard_map/dot_general | solution.py:83
  461.5 11.3 %convolution_convert_fusion = bf16[384,2048]{1,0:T(8,128)(2,1)} fusion(bf16[1408,2048]{1,0:T(8,128)(2,1)} %all-gather.13.cloned.1.call-done, bf16[2048,1408]{1,0:T(8,128)(2,1)} %all-gather.11.cloned.1.call-done, f32[384,1408]{1,0:T(8,128)} %convolution_multiply_fusion.1, f32[1408]{0:T(1024)S(1)} %copy-done.14, bf16[384,2048]{1,0:T(8,128)(2,1)S(1)} %copy-done.3, ...), kind=kOutput, calls=%fused_computation.22 | convolution fusion | flops 4436901888 | bytes 16858112 | tf_op jit(solution)/shard_map/dot_general | solution.py:86
  472.8 28.1 %reduce-scatter.5.cloned.1.call-done = bf16[384,512]{1,0:T(8,128)(2,1)} async-done(((bf16[384,2048]{1,0:T(8,128)(2,1)}), bf16[384,512]{1,0:T(8,128)(2,1)}) %reduce-scatter.5.cloned.1.call-update) | async-done | bytes 393232 | tf_op jit(solution)/shard_map/reduce_scatter | solution.py:19
  501.0 1.9 add_convert_fusion
  (78 shorter events, 5.2 us)
Async XLA Ops:
  6.5 24.7 %all-gather.7.cloned.1.call-start = ((), (), s32[]{:S(2)}) async-start(), calls=%async_computation.3 | async-start | bytes 1966080 | tf_op jit(solution)/shard_map/all_gather | solution.py:12
  7.3 118.5 %all-gather.9.cloned.1.call-start = ((), (), s32[]{:S(2)}) async-start(), calls=%async_computation.4 | async-start | bytes 6488064 | tf_op jit(solution)/shard_map/all_gather | solution.py:77
  9.6 208.9 %all-gather.11.cloned.1.call-start = ((), (), s32[]{:S(2)}) async-start(), calls=%async_computation.5 | async-start | bytes 6488064 | tf_op jit(solution)/shard_map/all_gather | solution.py:78
  10.7 115.1 %copy-start.11 = (f32[2048]{0:T(1024)S(1)}, f32[2048]{0:T(1024)}, u32[]{:S(2)}) copy-start(f32[2048]{0:T(1024)} %param.15) | copy-start | bytes 24580
  10.7 115.1 %copy-start.13 = (f32[1408]{0:T(1024)S(1)}, f32[1408]{0:T(1024)}, u32[]{:S(2)}) copy-start(f32[1408]{0:T(1024)} %param.19) | copy-start | bytes 16900
  10.7 301.1 %all-gather.13.cloned.1.call-start = ((), (), s32[]{:S(2)}) async-start(), calls=%async_computation.6 | async-start | bytes 6488064 | tf_op jit(solution)/shard_map/all_gather | solution.py:79
  12.2 337.1 %reduce-scatter.3.cloned.1.call-start = ((), (), s32[]{:S(2)}) async-start(), calls=%async_computation.7 | async-start | bytes 1966080 | tf_op jit(solution)/shard_map/reduce_scatter | solution.py:19
  33.1 278.7 %copy-start.2 = (bf16[384,2048]{1,0:T(8,128)(2,1)S(1)}, bf16[384,2048]{1,0:T(8,128)(2,1)}, u32[]{:S(2)}) copy-start(bf16[384,2048]{1,0:T(8,128)(2,1)} %all-gather.7.cloned.1.call-done) | copy-start | bytes 4718596
  33.1 278.7 %copy-start.14 = (f32[1408]{0:T(1024)S(1)}, f32[1408]{0:T(1024)}, u32[]{:S(2)}) copy-start(f32[1408]{0:T(1024)} %param.21) | copy-start | bytes 16900
  133.0 216.4 %copy-start.4 = (bf16[384,512]{1,0:T(8,128)(2,1)S(1)}, bf16[384,512]{1,0:T(8,128)(2,1)}, u32[]{:S(2)}) copy-start(bf16[384,512]{1,0:T(8,128)(2,1)} %param.14) | copy-start | bytes 1179652
  133.0 216.4 %copy-start.9 = (f32[512]{0:T(512)S(1)}, f32[512]{0:T(512)}, u32[]{:S(2)}) copy-start(f32[512]{0:T(512)} %param.23) | copy-start | bytes 6148
  323.0 28.3 %copy-start.7 = (f32[128,256]{1,0:T(8,128)S(1)}, f32[128,256]{1,0:T(8,128)}, u32[]{:S(2)}) copy-start(f32[128,256]{1,0:T(8,128)} %param.26) | copy-start | bytes 393220
  323.0 64.6 %copy-start.8 = (f32[256,128]{1,0:T(8,128)S(1)}, f32[256,128]{1,0:T(8,128)}, u32[]{:S(2)}) copy-start(f32[256,128]{1,0:T(8,128)} %param.24) | copy-start | bytes 393220
  323.0 96.3 %all-gather.15.cloned.1.call-start = ((), (), s32[]{:S(2)}) async-start(), calls=%async_computation.8 | async-start | bytes 1966080 | tf_op jit(solution)/shard_map/all_gather | solution.py:12
  383.1 38.0 %copy-start.12 = (f32[2048]{0:T(1024)S(1)}, f32[2048]{0:T(1024)}, u32[]{:S(2)}) copy-start(f32[2048]{0:T(1024)} %param.16) | copy-start | bytes 24580
  383.1 38.0 %copy-start.16 = (f32[128]{0:T(128)S(1)}, f32[128]{0:T(128)}, u32[]{:S(2)}) copy-start(f32[128]{0:T(128)} %param.25) | copy-start | bytes 1540
  384.1 46.5 %all-to-all-start = ((bf16[128,4,512]{2,0,1:T(8,128)(2,1)}), bf16[128,4,512]{2,0,1:T(8,128)(2,1)S(1)}, u32[]{:S(2)}, u32[]{:S(2)}) async-start(bf16[128,4,512]{2,0,1:T(8,128)(2,1)} %copy.17), calls=%async_computation.1 | async-start | bytes 1048576 | tf_op jit(solution)/shard_map/all_to_all | solution.py:96
  387.6 64.9 %all-gather.17.cloned.1.call-start = ((), (), s32[]{:S(2)}) async-start(), calls=%async_computation.9 | async-start | bytes 1966080 | tf_op jit(solution)/shard_map/all_gather | solution.py:12
  423.2 8.0 %copy-start = (bf16[384,512]{1,0:T(8,128)(2,1)S(1)}, bf16[384,512]{1,0:T(8,128)(2,1)}, u32[]{:S(2)}) copy-start(bf16[384,512]{1,0:T(8,128)(2,1)} %add_convert_fusion.2) | copy-start | bytes 1179652
  423.2 8.0 %copy-start.10 = (f32[512]{0:T(512)S(1)}, f32[512]{0:T(512)}, u32[]{:S(2)}) copy-start(f32[512]{0:T(512)} %param.27) | copy-start | bytes 6148
  431.2 23.0 %copy-start.15 = (f32[2048]{0:T(1024)S(1)}, f32[2048]{0:T(1024)}, u32[]{:S(2)}) copy-start(f32[2048]{0:T(1024)} %param.17) | copy-start | bytes 24580
  432.1 68.8 %reduce-scatter.5.cloned.1.call-start = ((), (), s32[]{:S(2)}) async-start(), calls=%async_computation.10 | async-start | bytes 1966080 | tf_op jit(solution)/shard_map/reduce_scatter | solution.py:19
  454.3 7.3 %copy-start.3 = (bf16[384,2048]{1,0:T(8,128)(2,1)S(1)}, bf16[384,2048]{1,0:T(8,128)(2,1)}, u32[]{:S(2)}) copy-start(bf16[384,2048]{1,0:T(8,128)(2,1)} %all-gather.17.cloned.1.call-done) | copy-start | bytes 4718596
  461.5 39.4 %copy-start.1 = (bf16[384,512]{1,0:T(8,128)(2,1)S(1)}, bf16[384,512]{1,0:T(8,128)(2,1)}, u32[]{:S(2)}) copy-start(bf16[384,512]{1,0:T(8,128)(2,1)} %add_convert_fusion.1) | copy-start | bytes 1179652
  (2 other events, 4.8 us)
Sparse Core Ops, SparseCore 0:
  8.9 22.3 all-gather.6
  33.5 92.2 all-gather.8
  128.0 90.4 all-gather.10
  220.4 91.2 all-gather.12
  323.1 26.1 reduce-scatter.2
  351.4 19.6 all-gather.14
  432.3 20.1 all-gather.16
  472.9 27.9 reduce-scatter.4
where the time goes:
time: 510 us
  waiting for transfers between devices  366 us (72%)
  blocking collectives  69.9 us (14%)
  matrix products  39.5 us (8%)
  other arithmetic  14.9 us (3%)
  between operations  13.8 us (3%)
    all_gather x1, waiting for transfers between devices, body(): lax.all_gather(down_half, 'fs', axis=1, tiled=True)  93.2 us
    all_gather x1, waiting for transfers between devices, body(): lax.all_gather(gate_half, 'fs', axis=0, tiled=True)  92.7 us
    all_gather x1, waiting for transfers between devices, body(): lax.all_gather(up_half, 'fs', axis=0, tiled=True)  85.6 us
    reduce_scatter x2, waiting for transfers between devices, residual_add(): lax.psum_scatter(partial_value.astype(jnp.bfloat16), 'tp', scatter_dimens...  54.4 us
    all_gather x3, waiting for transfers between devices, normed(): gathered = lax.all_gather(own_columns, 'tp', axis=1, tiled=True)  39.1 us
    all_gather x1, blocking collectives, body(): lax.all_gather(out_half, 'fs', axis=1, tiled=True)  31.7 us
    all_gather x1, blocking collectives, body(): lax.all_gather(in_half, 'fs', axis=0, tiled=True)  31.5 us
    dot_general x2, matrix products, feed_forward(): return jnp.dot(hidden, down_whole, preferred_element_type=jnp.float32)  22.5 us
  transfers between devices with their start and end apart: 9, of which 7 were waited for; matrix products, arithmetic and copies ran while one was open for 4% of the time, Pallas kernels for 0%

commit v1 on v0

--- a/solution.py
+++ b/solution.py
@@ -69,8 +69,11 @@
     down_half = down_weight.astype(jnp.bfloat16)
     in_half = pool_in_weight.astype(jnp.bfloat16)
     out_half = pool_out_weight.astype(jnp.bfloat16)
+    bind_corner = lambda d_out, vec, device_axis: jnp.concatenate(
+        lax.all_to_all(jnp.stack(lax.axis_size(device_axis) * [vec]), device_axis, 0, 0), axis=d_out
+    )
     in_whole, out_whole = (
-        lax.all_gather(in_half, "fs", axis=0, tiled=True),
+        bind_corner(0, in_half, "fs"),
         lax.all_gather(out_half, "fs", axis=1, tiled=True),
     )
     gate_whole, up_whole, down_whole = (

time: 510 us -> 490 us (0.961)
  blocking collectives: 69.9 us -> 48.6 us
  starting transfers between devices: 3.94 us -> 9.46 us
    all_gather x1 -> x0, blocking collectives: 31.5 us -> none  [body(): lax.all_gather(in_half, 'fs', axis=0, tiled=True)]
    all_gather x1, blocking collectives: 31.7 us -> 38.3 us  [body(): lax.all_gather(out_half, 'fs', axis=1, tiled=True)]
    all_to_all x0 -> x1, starting transfers between devices: none -> 5.5 us  [body(): lax.all_to_all(jnp.stack(lax.axis_size(device_axis) * [vec]), device_axis...]
  transfers between devices with their start and end apart: 9 -> 10, of which waited for: 7 -> 7; matrix products, arithmetic and copies ran while one was open for 4% -> 4% of each run, Pallas kernels for 0% -> 0%
where the time goes in v1:
time: 490 us; the launch traced here: 489 us
  waiting for transfers between devices  362 us (74%)
  blocking collectives  48.6 us (10%)
  matrix products  38.1 us (8%)
  other arithmetic  15 us (3%)
  between operations  13.8 us (3%)
  starting transfers between devices  9.46 us (2%)
    all_gather x1, waiting for transfers between devices, body(): lax.all_gather(down_half, 'fs', axis=1, tiled=True)  93.2 us
    all_gather x1, waiting for transfers between devices, body(): lax.all_gather(gate_half, 'fs', axis=0, tiled=True)  92.7 us
    all_gather x1, waiting for transfers between devices, body(): lax.all_gather(up_half, 'fs', axis=0, tiled=True)  85.6 us
    reduce_scatter x2, waiting for transfers between devices, residual_add(): lax.psum_scatter(partial_value.astype(jnp.bfloat16), 'tp', scatter_dimens...  54.5 us
    all_gather x1, blocking collectives, body(): lax.all_gather(out_half, 'fs', axis=1, tiled=True)  38.3 us
    all_gather x3, waiting for transfers between devices, normed(): gathered = lax.all_gather(own_columns, 'tp', axis=1, tiled=True)  34.9 us
    dot_general x2, matrix products, feed_forward(): return jnp.dot(hidden, down_whole, preferred_element_type=jnp.float32)  22.5 us
    dot_general x2, matrix products, feed_forward(): jnp.dot(normed_rows, gate_whole, preferred_element_type=jnp.float32)  14.4 us
  transfers between devices with their start and end apart: 10, of which 7 were waited for; matrix products, arithmetic and copies ran while one was open for 4% of the time, Pallas kernels for 0%

profile of v1, /device:TPU:0, one launch (start us, length us, event | category | flops | bytes accessed | tf_op | source)
XLA Modules:
  0.0 489.4 jit_solution(6346696547886097742)
XLA Ops:
  7.3 2.3 convert_element_type.144
  9.7 1.0 convert_element_type.145
  11.3 1.0 convert_element_type.147
  12.3 19.0 %all-gather.7.cloned.1.call-done = bf16[384,2048]{1,0:T(8,128)(2,1)} async-done(((bf16[384,512]{1,0:T(8,128)(2,1)}), bf16[384,2048]{1,0:T(8,128)(2,1)}) %all-gather.7.cloned.1.call-update) | async-done | bytes 1572880 | tf_op jit(solution)/shard_map/all_gather | solution.py:12
  31.3 1.8 fusion
  33.1 92.7 %all-gather.9.cloned.1.call-done = bf16[2048,1408]{1,0:T(8,128)(2,1)} async-done(((bf16[256,1408]{1,0:T(8,128)(2,1)}), bf16[2048,1408]{1,0:T(8,128)(2,1)}) %all-gather.9.cloned.1.call-update) | async-done | bytes 5767184 | tf_op jit(solution)/shard_map/all_gather | solution.py:80
  125.8 7.1 %convolution_multiply_fusion.3 = f32[384,1408]{1,0:T(8,128)} fusion(bf16[2048,1408]{1,0:T(8,128)(2,1)} %all-gather.9.cloned.1.call-done, f32[1408]{0:T(1024)S(1)} %copy-done.14, bf16[384,2048]{1,0:T(8,128)(2,1)} %all-gather.7.cloned.1.call-done, f32[2048]{0:T(1024)S(1)} %copy-done.12, f32[384]{0:T(512)S(1)} %add_rsqrt_fusion.2), kind=kOutput, calls=%fused_computation.21 | convolution fusion | flops 2218278912 | bytes 9518080 | tf_op jit(solution)/shard_map/dot_general | solution.py:86
  132.9 85.6 %all-gather.11.cloned.1.call-done = bf16[2048,1408]{1,0:T(8,128)(2,1)} async-done(((bf16[256,1408]{1,0:T(8,128)(2,1)}), bf16[2048,1408]{1,0:T(8,128)(2,1)}) %all-gather.11.cloned.1.call-update) | async-done | bytes 5767184 | tf_op jit(solution)/shard_map/all_gather | solution.py:81
  218.5 93.2 %all-gather.13.cloned.1.call-done = bf16[1408,2048]{1,0:T(8,128)(2,1)} async-done(((bf16[1408,256]{1,0:T(8,128)(2,1)}), bf16[1408,2048]{1,0:T(8,128)(2,1)}) %all-gather.13.cloned.1.call-update) | async-done | bytes 5767184 | tf_op jit(solution)/shard_map/all_gather | solution.py:82
  311.8 11.2 %convolution_convert_fusion.1 = bf16[384,2048]{1,0:T(8,128)(2,1)} fusion(bf16[1408,2048]{1,0:T(8,128)(2,1)} %all-gather.13.cloned.1.call-done, bf16[2048,1408]{1,0:T(8,128)(2,1)} %all-gather.11.cloned.1.call-done, f32[384,1408]{1,0:T(8,128)} %convolution_multiply_fusion.3, f32[1408]{0:T(1024)S(1)} %copy-done.15, bf16[384,2048]{1,0:T(8,128)(2,1)S(1)} %copy-done.3, ...), kind=kOutput, calls=%fused_computation.23 | convolution fusion | flops 4436901888 | bytes 16858112 | tf_op jit(solution)/shard_map/dot_general | solution.py:89
  323.1 26.3 %reduce-scatter.3.cloned.1.call-done = bf16[384,512]{1,0:T(8,128)(2,1)} async-done(((bf16[384,2048]{1,0:T(8,128)(2,1)}), bf16[384,512]{1,0:T(8,128)(2,1)}) %reduce-scatter.3.cloned.1.call-update) | async-done | bytes 393232 | tf_op jit(solution)/shard_map/reduce_scatter | solution.py:19
  349.4 1.9 add_convert_fusion.2
  352.2 5.5 %all-to-all-start = ((bf16[8,256,128]{2,1,0:T(8,128)(2,1)}), bf16[8,256,128]{2,1,0:T(8,128)(2,1)S(1)}, u32[]{:S(2)}, u32[]{:S(2)}) async-start(bf16[8,256,128]{2,1,0:T(8,128)(2,1)} %stack.2), calls=%async_computation.1 | async-start | bytes 1048576 | tf_op jit(solution)/shard_map/all_to_all | solution.py:73
  357.9 38.3 %all_gather.30 = bf16[128,2048]{0,1:T(8,128)(2,1)S(1)} all-gather(bf16[128,256]{0,1:T(8,128)(2,1)S(1)} %copy.16), channel_id=1, replica_groups=mesh['fs'=8,'tp'=4] {'fs'}, dimensions={1}, use_global_device_ids=true | all-gather | bytes 589824 | tf_op jit(solution)/shard_map/all_gather | solution.py:77
  396.2 1.0 copy.17
  397.3 1.9 fusion.3
  399.3 3.5 all-to-all-start.1
  404.2 10.3 %all_gather.29 = bf16[384,512]{0,1:T(8,128)(2,1)S(1)} all-gather(bf16[384,128]{0,1:T(8,128)(2,1)S(1)} %copy.15), channel_id=1, replica_groups=mesh['fs'=8,'tp'=4] {'tp'}, dimensions={1}, use_global_device_ids=true | all-gather | bytes 491520 | tf_op jit(solution)/shard_map/all_gather | solution.py:98
  416.3 15.9 %all-gather.17.cloned.1.call-done = bf16[384,2048]{1,0:T(8,128)(2,1)} async-done(((bf16[384,512]{1,0:T(8,128)(2,1)}), bf16[384,2048]{1,0:T(8,128)(2,1)}) %all-gather.17.cloned.1.call-update) | async-done | bytes 1572880 | tf_op jit(solution)/shard_map/all_gather | solution.py:12
  432.2 1.8 fusion.6
  434.0 7.2 %convolution_multiply_fusion.1 = f32[384,1408]{1,0:T(8,128)} fusion(bf16[2048,1408]{1,0:T(8,128)(2,1)} %all-gather.9.cloned.1.call-done, f32[1408]{0:T(1024)S(1)} %copy-done.14, bf16[384,2048]{1,0:T(8,128)(2,1)} %all-gather.17.cloned.1.call-done, f32[2048]{0:T(1024)S(1)} %copy-done.16, f32[384]{0:T(512)S(1)} %add_rsqrt_fusion), kind=kOutput, calls=%fused_computation.18 | convolution fusion | flops 2218278912 | bytes 9518080 | tf_op jit(solution)/shard_map/dot_general | solution.py:86
  441.2 11.3 %convolution_convert_fusion = bf16[384,2048]{1,0:T(8,128)(2,1)} fusion(bf16[1408,2048]{1,0:T(8,128)(2,1)} %all-gather.13.cloned.1.call-done, bf16[2048,1408]{1,0:T(8,128)(2,1)} %all-gather.11.cloned.1.call-done, f32[384,1408]{1,0:T(8,128)} %convolution_multiply_fusion.1, f32[1408]{0:T(1024)S(1)} %copy-done.15, bf16[384,2048]{1,0:T(8,128)(2,1)S(1)} %copy-done.4, ...), kind=kOutput, calls=%fused_computation.22 | convolution fusion | flops 4436901888 | bytes 16858112 | tf_op jit(solution)/shard_map/dot_general | solution.py:89
  452.5 28.2 %reduce-scatter.5.cloned.1.call-done = bf16[384,512]{1,0:T(8,128)(2,1)} async-done(((bf16[384,2048]{1,0:T(8,128)(2,1)}), bf16[384,512]{1,0:T(8,128)(2,1)}) %reduce-scatter.5.cloned.1.call-update) | async-done | bytes 393232 | tf_op jit(solution)/shard_map/reduce_scatter | solution.py:19
  480.7 1.9 add_convert_fusion
  (82 shorter events, 5.7 us)
Async XLA Ops:
  6.5 24.7 %all-gather.7.cloned.1.call-start = ((), (), s32[]{:S(2)}) async-start(), calls=%async_computation.4 | async-start | bytes 1966080 | tf_op jit(solution)/shard_map/all_gather | solution.py:12
  7.3 118.5 %all-gather.9.cloned.1.call-start = ((), (), s32[]{:S(2)}) async-start(), calls=%async_computation.5 | async-start | bytes 6488064 | tf_op jit(solution)/shard_map/all_gather | solution.py:80
  9.7 208.9 %all-gather.11.cloned.1.call-start = ((), (), s32[]{:S(2)}) async-start(), calls=%async_computation.6 | async-start | bytes 6488064 | tf_op jit(solution)/shard_map/all_gather | solution.py:81
  10.7 115.1 %copy-start.12 = (f32[2048]{0:T(1024)S(1)}, f32[2048]{0:T(1024)}, u32[]{:S(2)}) copy-start(f32[2048]{0:T(1024)} %param.15) | copy-start | bytes 24580
  10.7 115.1 %copy-start.14 = (f32[1408]{0:T(1024)S(1)}, f32[1408]{0:T(1024)}, u32[]{:S(2)}) copy-start(f32[1408]{0:T(1024)} %param.19) | copy-start | bytes 16900
  10.7 301.0 %all-gather.13.cloned.1.call-start = ((), (), s32[]{:S(2)}) async-start(), calls=%async_computation.7 | async-start | bytes 6488064 | tf_op jit(solution)/shard_map/all_gather | solution.py:82
  12.2 337.2 %reduce-scatter.3.cloned.1.call-start = ((), (), s32[]{:S(2)}) async-start(), calls=%async_computation.8 | async-start | bytes 1966080 | tf_op jit(solution)/shard_map/reduce_scatter | solution.py:19
  33.1 278.7 %copy-start.3 = (bf16[384,2048]{1,0:T(8,128)(2,1)S(1)}, bf16[384,2048]{1,0:T(8,128)(2,1)}, u32[]{:S(2)}) copy-start(bf16[384,2048]{1,0:T(8,128)(2,1)} %all-gather.7.cloned.1.call-done) | copy-start | bytes 4718596
  33.1 278.7 %copy-start.15 = (f32[1408]{0:T(1024)S(1)}, f32[1408]{0:T(1024)}, u32[]{:S(2)}) copy-start(f32[1408]{0:T(1024)} %param.21) | copy-start | bytes 16900
  132.9 216.5 %copy-start.5 = (bf16[384,512]{1,0:T(8,128)(2,1)S(1)}, bf16[384,512]{1,0:T(8,128)(2,1)}, u32[]{:S(2)}) copy-start(bf16[384,512]{1,0:T(8,128)(2,1)} %param.14) | copy-start | bytes 1179652
  132.9 216.5 %copy-start.10 = (f32[512]{0:T(512)S(1)}, f32[512]{0:T(512)}, u32[]{:S(2)}) copy-start(f32[512]{0:T(512)} %param.23) | copy-start | bytes 6148
  323.0 28.3 %copy-start.8 = (f32[256,128]{1,0:T(8,128)S(1)}, f32[256,128]{1,0:T(8,128)}, u32[]{:S(2)}) copy-start(f32[256,128]{1,0:T(8,128)} %param.24) | copy-start | bytes 393220
  323.0 34.7 %copy-start.9 = (f32[128,256]{1,0:T(8,128)S(1)}, f32[128,256]{1,0:T(8,128)}, u32[]{:S(2)}) copy-start(f32[128,256]{1,0:T(8,128)} %param.26) | copy-start | bytes 393220
  323.0 74.3 %all-gather.15.cloned.1.call-start = ((), (), s32[]{:S(2)}) async-start(), calls=%async_computation.9 | async-start | bytes 1966080 | tf_op jit(solution)/shard_map/all_gather | solution.py:12
  352.2 47.0 %all-to-all-start = ((bf16[8,256,128]{2,1,0:T(8,128)(2,1)}), bf16[8,256,128]{2,1,0:T(8,128)(2,1)S(1)}, u32[]{:S(2)}, u32[]{:S(2)}) async-start(bf16[8,256,128]{2,1,0:T(8,128)(2,1)} %stack.2), calls=%async_computation.1 | async-start | bytes 1048576 | tf_op jit(solution)/shard_map/all_to_all | solution.py:73
  357.8 44.9 %copy-start.13 = (f32[2048]{0:T(1024)S(1)}, f32[2048]{0:T(1024)}, u32[]{:S(2)}) copy-start(f32[2048]{0:T(1024)} %param.16) | copy-start | bytes 24580
  357.9 44.9 %copy-start.17 = (f32[128]{0:T(128)S(1)}, f32[128]{0:T(128)}, u32[]{:S(2)}) copy-start(f32[128]{0:T(128)} %param.25) | copy-start | bytes 1540
  399.3 15.2 %all-to-all-start.1 = ((bf16[128,4,512]{2,0,1:T(8,128)(2,1)}), bf16[128,4,512]{2,0,1:T(8,128)(2,1)S(1)}, u32[]{:S(2)}, u32[]{:S(2)}) async-start(bf16[128,4,512]{2,0,1:T(8,128)(2,1)} %copy.17), calls=%async_computation.2 | async-start | bytes 1048576 | tf_op jit(solution)/shard_map/all_to_all | solution.py:99
  402.7 29.4 %all-gather.17.cloned.1.call-start = ((), (), s32[]{:S(2)}) async-start(), calls=%async_computation.10 | async-start | bytes 1966080 | tf_op jit(solution)/shard_map/all_gather | solution.py:12
  403.5 11.6 %copy-start = (bf16[384,512]{1,0:T(8,128)(2,1)S(1)}, bf16[384,512]{1,0:T(8,128)(2,1)}, u32[]{:S(2)}) copy-start(bf16[384,512]{1,0:T(8,128)(2,1)} %add_convert_fusion.2) | copy-start | bytes 1179652
  403.5 11.6 %copy-start.11 = (f32[512]{0:T(512)S(1)}, f32[512]{0:T(512)}, u32[]{:S(2)}) copy-start(f32[512]{0:T(512)} %param.27) | copy-start | bytes 6148
  415.1 18.8 %copy-start.16 = (f32[2048]{0:T(1024)S(1)}, f32[2048]{0:T(1024)}, u32[]{:S(2)}) copy-start(f32[2048]{0:T(1024)} %param.17) | copy-start | bytes 24580
  416.0 64.6 %reduce-scatter.5.cloned.1.call-start = ((), (), s32[]{:S(2)}) async-start(), calls=%async_computation.11 | async-start | bytes 1966080 | tf_op jit(solution)/shard_map/reduce_scatter | solution.py:19
  441.2 39.5 %copy-start.1 = (bf16[384,512]{1,0:T(8,128)(2,1)S(1)}, bf16[384,512]{1,0:T(8,128)(2,1)}, u32[]{:S(2)}) copy-start(bf16[384,512]{1,0:T(8,128)(2,1)} %add_convert_fusion.1) | copy-start | bytes 1179652
  (4 other events, 17.5 us)
Sparse Core Ops, SparseCore 0:
  8.9 22.3 all-gather.6
  33.5 92.2 all-gather.8
  128.0 90.4 all-gather.10
  220.4 91.2 all-gather.12
  323.2 26.2 reduce-scatter.2
  351.5 19.6 all-gather.14
  416.2 15.9 all-gather.16
  452.6 28.0 reduce-scatter.4
